TPU v7x, 32 devices: a whole 2x2x4 slice. The times are simulated.
32 devices in a mesh: sp: 8 (over z, y), tp: 4 (over x, core).
Axes of the slice: x: 2, y: 2, z: 4, core: 2. Of those that a mesh axis runs over, the one named last changes fastest.
Arguments:
- tokens: bfloat16 [2048, 1024], P(('sp', 'tp')), may hold values from -7.5 to 7.5, as said below
- query_weight: bfloat16 [1024, 2048], P('sp', 'tp'), may hold values from -0.1875 to 0.1875
- key_weight: bfloat16 [1024, 2048], P('sp', 'tp'), may hold values from -0.1875 to 0.1875
- value_weight: bfloat16 [1024, 2048], P('sp', 'tp'), may hold values from -0.1875 to 0.1875
- gate_weight: bfloat16 [1024, 16], P('sp', 'tp'), may hold values from -0.1875 to 0.1875
- forget_bias: float32 [16], P('tp'), may hold values from 0 to 2
- out_weight: bfloat16 [2048, 1024], P('tp', 'sp'), may hold values from -0.125 to 0.125
- out_gain: float32 [1024], replicated, may hold values from 0.5 to 1.5
Outputs:
- mixed: bfloat16 [2048, 1024], P(('sp', 'tp'))
Inputs may be any that keep to these rules, and one draw needn't show every extreme that they name: `tokens`: each entry is a bounded noise value (at most 6 in size) plus an offset in -1.5 to 1.5 shared by the 256 rows of one index of sp, so every entry lies within -7.5 and 7.5.
All inputs are finite; a program needn't handle non-finite values.
Results may differ from a plain program's by a relative error of at most 0.006.
Values may be sent and summed in bfloat16 or wider, within the bound.
A program may use at most 128 MiB of HBM per device.

v0:
```python
import math

import jax
import jax.numpy as jnp
from jax import lax
from jax.sharding import PartitionSpec as P


def on_whole(shard, axis, dim, block):
    whole = lax.all_gather(shard, axis, axis=dim, tiled=True)
    return block(whole, jnp.int32(0))


def over_all(shard, axis, dim, absorb, state):
    everything = jax.tree.map(lambda a: lax.all_gather(a, axis, axis=dim, tiled=True), shard)
    return absorb(state, everything, jnp.int32(0))


def own_rows(product, width, axis):
    everything = product(jnp.int32(0), lax.axis_size(axis) * width)
    own = lax.psum_scatter(everything, axis, scatter_dimension=0, tiled=True)
    return own


def on_device(
    tokens, query_weight, key_weight, value_weight, gate_weight, forget_bias, out_weight, out_gain
):
    width = query_weight.shape[1]
    heads = gate_weight.shape[1]
    head_size = width // heads
    whole_q = lax.all_gather(query_weight, "sp", axis=0, tiled=True)
    whole_k = lax.all_gather(key_weight, "sp", axis=0, tiled=True)
    whole_v = lax.all_gather(value_weight, "sp", axis=0, tiled=True)
    whole_g = lax.all_gather(gate_weight, "sp", axis=0, tiled=True)
    joined = jnp.concatenate([whole_q, whole_k, whole_v, whole_g], axis=1)

    def project(piece, start):
        return jnp.dot(piece, joined, preferred_element_type=jnp.float32)

    projected = on_whole(tokens, "tp", 0, project)
    block = projected.shape[0]
    queries = projected[:, :width].astype(jnp.bfloat16).reshape(block, heads, head_size)
    keys = projected[:, width : 2 * width].astype(jnp.bfloat16).reshape(block, heads, head_size)
    values = (
        projected[:, 2 * width : 3 * width].astype(jnp.bfloat16).reshape(block, heads, head_size)
    )
    seq_len = block * lax.axis_size("sp")
    log_gate = jax.nn.log_sigmoid(projected[:, 3 * width :] + forget_bias + math.log(seq_len))
    gates_all = lax.all_gather(log_gate, "sp", axis=0, tiled=True)
    cumulative = jnp.cumsum(gates_all, axis=0)
    first = lax.axis_index("sp") * block
    query_cum = lax.dynamic_slice_in_dim(cumulative, first, block, 0)
    query_pos = first + jnp.arange(block, dtype=jnp.int32)
    scale = head_size ** (-0.5)

    def update(carry, piece, start):
        run_max, run_sum, run_acc = carry
        key_piece, value_piece = piece
        length = key_piece.shape[0]
        key_cum = lax.dynamic_slice_in_dim(cumulative, start, length, 0)
        logits = (
            jnp.einsum("qhd,khd->hqk", queries, key_piece, preferred_element_type=jnp.float32)
            * scale
        )
        logits = logits + query_cum.T[:, :, None] - key_cum.T[:, None, :]
        key_pos = start + jnp.arange(length, dtype=jnp.int32)
        allowed = (key_pos[None, :] <= query_pos[:, None])[None]
        logits = jnp.where(allowed, logits, -1e30)
        new_max = jnp.maximum(run_max, jnp.max(logits, axis=-1))
        probs = jnp.where(allowed, jnp.exp(logits - new_max[..., None]), 0.0)
        factor = jnp.exp(run_max - new_max)
        new_sum = run_sum * factor + jnp.sum(probs, axis=-1)
        new_acc = run_acc * factor[..., None] + jnp.einsum(
            "hqk,khd->hqd", probs, value_piece.astype(jnp.float32)
        )
        return (new_max, new_sum, new_acc)

    def attend(carry, piece, start):
        return lax.cond(
            start > first + block - 1,
            lambda state: state,
            lambda state: update(state, piece, start),
            carry,
        )

    initial = (
        jnp.full((heads, block), -1e30, jnp.float32),
        jnp.zeros((heads, block), jnp.float32),
        jnp.zeros((heads, block, head_size), jnp.float32),
    )
    run_max, run_sum, run_acc = over_all((keys, values), "sp", 0, attend, initial)
    attended = (
        (run_acc / run_sum[..., None]).transpose(1, 0, 2).reshape(block, width).astype(jnp.bfloat16)
    )
    out_full = lax.all_gather(out_weight, "sp", axis=1, tiled=True)
    rows = tokens.shape[0]

    def term(start, count):
        return jnp.dot(
            lax.dynamic_slice_in_dim(attended, start, count, 0),
            out_full,
            preferred_element_type=jnp.float32,
        )

    summed = own_rows(term, rows, "tp")
    normed = summed * lax.rsqrt(jnp.mean(summed * summed, axis=-1, keepdims=True) + 1e-06)
    return (normed * out_gain).astype(jnp.bfloat16)


def solution(mesh):
    placed = (
        P(("sp", "tp"), None),
        P("sp", "tp"),
        P("sp", "tp"),
        P("sp", "tp"),
        P("sp", "tp"),
        P("tp"),
        P("tp", "sp"),
        P(),
    )
    return jax.shard_map(
        on_device, mesh=mesh, in_specs=placed, out_specs=P(("sp", "tp"), None), check_vma=False
    )
```

profile of v0, /device:TPU:25, one launch (start us, length us, event | category | flops | bytes accessed | tf_op | source)
XLA Modules:
  0.0 312.2 jit_solution(10969626571004091959)
XLA Ops:
  6.5 0.0 all-gather.11.cloned.1.call-start
  6.5 0.7 all-gather.11.cloned.1.call-update
  7.3 0.0 all-gather.9.cloned.1.call-start
  7.3 0.7 all-gather.9.cloned.1.call-update
  8.0 0.0 all-gather.7.cloned.1.call-start
  8.1 0.7 all-gather.7.cloned.1.call-update
  8.7 0.0 all-gather.13.cloned.1.call-start
  8.8 13.2 %all_gather.30 = bf16[1024,4]{0,1:T(4,128)(2,1)S(1)} all-gather(bf16[128,4]{0,1:T(4,128)(2,1)} %param.14), channel_id=1, replica_groups=mesh['sp'=8,'tp'=4] {'sp'}, dimensions={0}, use_global_device_ids=true | all-gather | bytes 9216 | tf_op jit(solution)/shard_map/all_gather | solution.py:34
  21.9 0.2 copy.14
  22.1 11.0 %all_gather.31 = bf16[256,1024]{1,0:T(8,128)(2,1)S(1)} all-gather(bf16[64,1024]{1,0:T(8,128)(2,1)} %param.10), channel_id=1, replica_groups=mesh['sp'=8,'tp'=4] {'tp'}, dimensions={0}, use_global_device_ids=true | all-gather | bytes 655360 | tf_op jit(solution)/shard_map/all_gather | solution.py:10
  33.1 0.0 copy-start.1
  33.1 14.3 %all-gather.11.cloned.1.call-done = bf16[1024,512]{1,0:T(8,128)(2,1)} async-done(((bf16[128,512]{1,0:T(8,128)(2,1)}), bf16[1024,512]{1,0:T(8,128)(2,1)}) %all-gather.11.cloned.1.call-update) | async-done | bytes 1048592 | tf_op jit(solution)/shard_map/all_gather | solution.py:33
  47.4 41.3 %all-gather.9.cloned.1.call-done = bf16[1024,512]{1,0:T(8,128)(2,1)} async-done(((bf16[128,512]{1,0:T(8,128)(2,1)}), bf16[1024,512]{1,0:T(8,128)(2,1)}) %all-gather.9.cloned.1.call-update) | async-done | bytes 1048592 | tf_op jit(solution)/shard_map/all_gather | solution.py:32
  88.7 41.3 %all-gather.7.cloned.1.call-done = bf16[1024,512]{1,0:T(8,128)(2,1)} async-done(((bf16[128,512]{1,0:T(8,128)(2,1)}), bf16[1024,512]{1,0:T(8,128)(2,1)}) %all-gather.7.cloned.1.call-update) | async-done | bytes 1048592 | tf_op jit(solution)/shard_map/all_gather | solution.py:31
  129.9 2.9 fusion.32
  132.9 0.9 copy.15
  133.8 0.0 all-gather.13.cloned.1.call-update
  133.8 0.0 all-gather.15.cloned.1.call-start
  133.9 0.8 copy.16
  134.7 0.0 all-gather.15.cloned.1.call-update
  134.7 0.0 all-gather.17.cloned.1.call-start
  134.8 0.5 all-gather.17.cloned.1.call-update
  135.3 0.0 reduce-scatter.2.cloned.1.call-start
  135.4 0.0 copy-done.1
  135.4 0.1 fusion.26
  135.5 22.8 %all_gather.33 = f32[2048,4]{0,1:T(4,128)S(1)} all-gather(f32[256,4]{0,1:T(4,128)S(1)} %fusion.26), channel_id=1, replica_groups=mesh['sp'=8,'tp'=4] {'sp'}, dimensions={0}, use_global_device_ids=true | all-gather | bytes 36864 | tf_op jit(solution)/shard_map/all_gather | solution.py:49
  158.3 1.1 reduce-window.6
  159.4 0.2 slice_reduce_fusion
  159.6 0.2 reduce-window.9
  159.8 0.1 add_bitcast_fusion
  159.9 23.7 %all-gather.13.cloned.1.call-done = bf16[2048,4,128]{2,0,1:T(8,128)(2,1)} async-done(((bf16[256,4,128]{2,0,1:T(8,128)(2,1)}), bf16[2048,4,128]{2,0,1:T(8,128)(2,1)}) %all-gather.13.cloned.1.call-update) | async-done | bytes 2097168 | tf_op jit(solution)/shard_map/all_gather | solution.py:15
  183.6 50.1 %all-gather.15.cloned.1.call-done = bf16[2048,4,128]{2,0,1:T(8,128)(2,1)} async-done(((bf16[256,4,128]{2,0,1:T(8,128)(2,1)}), bf16[2048,4,128]{2,0,1:T(8,128)(2,1)}) %all-gather.15.cloned.1.call-update) | async-done | bytes 2097168 | tf_op jit(solution)/shard_map/all_gather | solution.py:15
  233.7 0.0 copy-start
  233.7 11.8 %conditional.1 = (f32[4,256]{1,0:T(4,128)S(1)}, f32[4,256,128]{1,2,0:T(8,128)S(1)}) conditional(s32[]{:T(128)} %convert_element_type.19, (s32[]{:T(128)}, s32[256]{0:T(256)S(1)}, bf16[256,1540]{0,1:T(8,128)(2,1)S(1)}, bf16[2048,4,128]{2,0,1:T(8,128)(2,1)}, f32[256,4]{0,1:T(4,128)S(1)}, /*index=5*/f32[2048,4]{0,1:T(4,128)S(1)}, ...), branch_computations={%region_2.5_spmd, %region_5.6_spmd} | conditional | flops 1112149248 | bytes 42363952 | solution.py:79
  233.7 0.4 iota_compare_fusion
  234.1 0.0 copy-start.2
  234.1 4.6 %fusion.2 = (f32[4,256]{1,0:T(4,128)S(1)}, f32[4,256,2048]{2,1,0:T(8,128)S(1)}) fusion(f32[4,2048]{1,0:T(4,128)S(1)} %bitcast.40, f32[4,256]{1,0:T(4,128)S(1)} %bitcast.45, pred[256,2048]{1,0:T(8,128)(4,1)S(1)} %iota_compare_fusion, bf16[256,4,128]{0,2,1:T(8,128)(2,1)S(1)} %bitcast.37, bf16[2048,4,128]{2,0,1:T(8,128)(2,1)} %get-tuple-element.25), kind=kOutput, calls=%fused_computation.4 | convolution fusion | flops 547355648 | bytes 11313152 | tf_op jit(solution)/shard_map/cond/branch_0_fun/qhd,khd->hqk/dot_general | solution.py:62
  238.8 3.2 %fusion.1 = f32[4,256]{1,0:T(4,128)S(1)} fusion(f32[4,256,2048]{2,1,0:T(8,128)S(1)} %get-tuple-element.45, f32[4,256]{1,0:T(4,128)S(1)} %broadcast_maximum_fusion, f32[4,2048]{1,0:T(4,128)S(1)} %bitcast.41, f32[4,256]{1,0:T(4,128)S(1)} %bitcast.46, pred[256,2048]{1,0:T(8,128)(4,1)S(1)} %iota_compare_fusion), kind=kLoop, calls=%fused_computation.3 | loop fusion | flops 14679040 | bytes 8957952 | tf_op jit(solution)/shard_map/cond/branch_0_fun/reduce_sum | solution.py:72
  242.0 0.0 copy-done.2
  242.0 3.3 %fusion.10 = f32[4,256,128]{2,1,0:T(8,128)S(1)} fusion(bf16[2048,4,128]{2,0,1:T(8,128)(2,1)S(1)} %copy-done.2, f32[4,256,2048]{2,1,0:T(8,128)S(1)} %get-tuple-element.45, f32[4,256]{1,0:T(4,128)S(1)} %broadcast_maximum_fusion, f32[4,2048]{1,0:T(4,128)S(1)} %bitcast.42, f32[4,256]{1,0:T(4,128)S(1)} %bitcast.47, pred[256,2048]{1,0:T(8,128)(4,1)S(1)} %iota_compare_fusion, ...), kind=kOutput, calls=%fused_computation.13 | convolution fusion | flops 549584896 | bytes 11579392 | tf_op jit(solution)/shard_map/cond/branch_0_fun/hqk,khd->hqd/dot_general | solution.py:73
  245.2 0.2 copy.19
  245.5 27.1 %all-gather.17.cloned.1.call-done = bf16[512,1024]{1,0:T(8,128)(2,1)} async-done(((bf16[512,128]{1,0:T(8,128)(2,1)}), bf16[512,1024]{1,0:T(8,128)(2,1)}) %all-gather.17.cloned.1.call-update) | async-done | bytes 1048592 | tf_op jit(solution)/shard_map/all_gather | solution.py:95
  272.6 2.7 fusion.33
  275.3 0.0 reduce-scatter.2.cloned.1.call-update
  275.3 27.2 %reduce-scatter.2.cloned.1.call-done = f32[64,1024]{1,0:T(8,128)} async-done(((f32[256,1024]{1,0:T(8,128)}), f32[64,1024]{1,0:T(8,128)}) %reduce-scatter.2.cloned.1.call-update) | async-done | bytes 262160 | tf_op jit(solution)/shard_map/reduce_scatter | solution.py:21
  302.6 1.1 multiply_reduce_fusion
  303.6 0.0 copy-done
  303.6 1.7 multiply_convert_fusion
  (11 shorter events, 0.2 us)
Async XLA Ops:
  6.5 40.9 %all-gather.11.cloned.1.call-start = ((), (), s32[]{:S(2)}) async-start(), calls=%async_computation.3 | async-start | bytes 1179648 | tf_op jit(solution)/shard_map/all_gather | solution.py:33
  7.3 81.4 %all-gather.9.cloned.1.call-start = ((), (), s32[]{:S(2)}) async-start(), calls=%async_computation.2 | async-start | bytes 1179648 | tf_op jit(solution)/shard_map/all_gather | solution.py:32
  8.0 121.9 %all-gather.7.cloned.1.call-start = ((), (), s32[]{:S(2)}) async-start(), calls=%async_computation.1 | async-start | bytes 1179648 | tf_op jit(solution)/shard_map/all_gather | solution.py:31
  8.7 174.9 %all-gather.13.cloned.1.call-start = ((), (), s32[]{:S(2)}) async-start(), calls=%async_computation.4 | async-start | bytes 2359296 | tf_op jit(solution)/shard_map/all_gather | solution.py:15
  33.1 102.2 %copy-start.1 = (f32[4]{0:T(128)S(1)}, f32[4]{0:T(128)}, u32[]{:S(2)}) copy-start(f32[4]{0:T(128)} %param.15) | copy-start | bytes 52
  133.8 99.9 %all-gather.15.cloned.1.call-start = ((), (), s32[]{:S(2)}) async-start(), calls=%async_computation.5 | async-start | bytes 2359296 | tf_op jit(solution)/shard_map/all_gather | solution.py:15
  134.7 137.9 %all-gather.17.cloned.1.call-start = ((), (), s32[]{:S(2)}) async-start(), calls=%async_computation.6 | async-start | bytes 1179648 | tf_op jit(solution)/shard_map/all_gather | solution.py:95
  135.3 167.3 %reduce-scatter.2.cloned.1.call-start = ((), (), s32[]{:S(2)}) async-start(), calls=%async_computation.7 | async-start | bytes 1310720 | tf_op jit(solution)/shard_map/reduce_scatter | solution.py:21
  233.7 70.0 %copy-start = (f32[1024]{0:T(1024)S(1)}, f32[1024]{0:T(1024)}, u32[]{:S(2)}) copy-start(f32[1024]{0:T(1024)} %param.17) | copy-start | bytes 12292
  234.1 7.9 %copy-start.2 = (bf16[2048,4,128]{2,0,1:T(8,128)(2,1)S(1)}, bf16[2048,4,128]{2,0,1:T(8,128)(2,1)}, u32[]{:S(2)}) copy-start(bf16[2048,4,128]{2,0,1:T(8,128)(2,1)} %get-tuple-element.28) | copy-start | bytes 6291460 | tf_op jit(solution)/shard_map/cond
Sparse Core Ops, SparseCore 0:
  9.5 37.8 all-gather.10
  49.5 39.0 all-gather.8
  90.8 39.0 all-gather.6
  133.9 49.6 all-gather.12
  185.6 47.9 all-gather.14
  235.6 36.9 all-gather.16
  275.4 27.0 reduce-scatter.1
where the time goes:
time: 314 us; the launch traced here: 312 us
  waiting for transfers between devices  228 us (73%)
  blocking collectives  46.9 us (15%)
  between operations  13.6 us (4%)
  matrix products  13.5 us (4%)
  other arithmetic  7.89 us (3%)
    all_gather x2, waiting for transfers between devices, over_all(): lax.all_gather(a, axis, axis=dim, tiled=True)  73.8 us
    all_gather x1, waiting for transfers between devices, on_device(): whole_q = lax.all_gather(query_weight, 'sp', axis=0, tiled=True)  41.3 us
    all_gather x1, waiting for transfers between devices, on_device(): whole_k = lax.all_gather(key_weight, 'sp', axis=0, tiled=True)  41.3 us
    reduce_scatter x1, waiting for transfers between devices, own_rows(): own = lax.psum_scatter(everything, axis, scatter_dimension=0, tiled=True)  27.2 us
    all_gather x1, waiting for transfers between devices, on_device(): out_full = lax.all_gather(out_weight, 'sp', axis=1, tiled=True)  27.1 us
    all_gather x1, blocking collectives, on_device(): gates_all = lax.all_gather(log_gate, 'sp', axis=0, tiled=True)  22.8 us
    all_gather x1, waiting for transfers between devices, on_device(): whole_v = lax.all_gather(value_weight, 'sp', axis=0, tiled=True)  14.3 us
    all_gather x1, blocking collectives, on_device(): whole_g = lax.all_gather(gate_weight, 'sp', axis=0, tiled=True)  13.2 us
  transfers between devices with their start and end apart: 7, of which 7 were waited for; matrix products, arithmetic and copies ran while one was open for 5% of the time, Pallas kernels for 0%

commit v1 on v0

--- a/solution.py
+++ b/solution.py
@@ -3,6 +3,8 @@
 import jax
 import jax.numpy as jnp
 from jax import lax
+from jax.experimental import pallas as pl
+from jax.experimental.pallas import tpu as pltpu
 from jax.sharding import PartitionSpec as P
 
 
@@ -107,6 +109,406 @@
     return (normed * out_gain).astype(jnp.bfloat16)
 
 
+MESH = pl.DeviceIdType.MESH
+Z_, X_, Y_, DA, DB, PC, PX, PY, PA, PB = range(10)
+
+
+def rdma(src, dst, send, recv, sp, tp):
+    return pltpu.make_async_remote_copy(
+        src_ref=src,
+        dst_ref=dst,
+        send_sem=send,
+        recv_sem=recv,
+        device_id={"sp": sp, "tp": tp},
+        device_id_type=MESH,
+    )
+
+
+class Place:
+    def __init__(self, depth):
+        sp, tp = lax.axis_index("sp"), lax.axis_index("tp")
+        self.depth, self.sp, self.tp = depth, sp, tp
+        self.z, self.y = sp // 2, lax.rem(sp, 2)
+        self.x, self.c = tp // 2, lax.rem(tp, 2)
+
+    def back(self, j):
+        return lax.rem(self.z + self.depth - j, self.depth)
+
+    def ahead(self, j):
+        return lax.rem(self.z + j, self.depth)
+
+
+class Gather:
+    def __init__(self, at, own, buf, send, recv, local):
+        self.at, self.own, self.buf = at, own, buf
+        self.send, self.recv, self.local = send, recv, local
+        self.rows = own.shape[0]
+        self.sent = []
+
+    def block(self, z, y, x, c, half=None):
+        start = (((z * 2 + y) * 2 + x) * 2 + c) * self.rows
+        size = self.rows
+        if half is not None:
+            size = self.rows // 2
+            start = start + half * size
+        return self.buf.at[pl.ds(pl.multiple_of(start, size), size)]
+
+    def go(self, kind, j, dst, sp, tp, src=None):
+        copy = rdma(
+            dst if src is None else src,
+            dst,
+            self.send.at[kind, j],
+            self.recv.at[kind, j],
+            sp,
+            tp,
+        )
+        copy.start()
+        self.sent.append(copy)
+
+    def arrived(self, kind, j, ref):
+        pltpu.make_async_copy(ref, ref, self.recv.at[kind, j]).wait()
+
+    def to_x(self, kind, j, ref, src=None):
+        a = self.at
+        self.go(kind, j, ref, a.sp, (1 - a.x) * 2 + a.c, src)
+
+    def to_y(self, kind, j, ref, src=None):
+        a = self.at
+        self.go(kind, j, ref, a.z * 2 + 1 - a.y, a.tp, src)
+
+    def to_core(self, kind, j, ref, src=None):
+        a = self.at
+        self.go(kind, j, ref, a.sp, a.x * 2 + 1 - a.c, src)
+
+    def begin(self):
+        a = self.at
+        mine = self.block(a.z, a.y, a.x, a.c)
+        self.keep = pltpu.make_async_copy(self.own, mine, self.local)
+        self.keep.start()
+        self.to_x(X_, 0, mine, self.own)
+        self.to_y(Y_, 0, mine, self.own)
+        for j in range(1, a.depth):
+            self.go(Z_, j, mine, a.ahead(j) * 2 + a.y, a.tp, self.own)
+        self.to_core(PC, 0, mine, self.own)
+
+    def column(self, j):
+        a = self.at
+        ref = self.block(a.back(j), a.y, a.x, a.c)
+        self.arrived(Z_, j, ref)
+        self.to_x(X_, j, ref)
+        self.to_y(Y_, j, ref)
+        self.to_core(PC, j, ref)
+
+    def sides(self, j):
+        a = self.at
+        z = a.back(j)
+        ref = self.block(z, a.y, 1 - a.x, a.c)
+        self.arrived(X_, j, ref)
+        self.to_y(DA, j, self.block(z, a.y, 1 - a.x, a.c, 0))
+        self.to_core(PX, j, ref)
+        ref = self.block(z, 1 - a.y, a.x, a.c)
+        self.arrived(Y_, j, ref)
+        self.to_x(DB, j, self.block(z, 1 - a.y, a.x, a.c, 1))
+        self.to_core(PY, j, ref)
+
+    def corner(self, j):
+        a = self.at
+        z = a.back(j)
+        for kind, onward, half in ((DA, PA, 0), (DB, PB, 1)):
+            ref = self.block(z, 1 - a.y, 1 - a.x, a.c, half)
+            self.arrived(kind, j, ref)
+            self.to_core(onward, j, ref)
+
+    def partner(self, j):
+        a = self.at
+        z, c = a.back(j), 1 - a.c
+        self.arrived(PC, j, self.block(z, a.y, a.x, c))
+        self.arrived(PX, j, self.block(z, a.y, 1 - a.x, c))
+        self.arrived(PY, j, self.block(z, 1 - a.y, a.x, c))
+        self.arrived(PA, j, self.block(z, 1 - a.y, 1 - a.x, c, 0))
+        self.arrived(PB, j, self.block(z, 1 - a.y, 1 - a.x, c, 1))
+
+    def end(self):
+        self.keep.wait()
+        for copy in self.sent:
+            copy.wait_send()
+
+
+def layer(
+    depth, size, tok_ref, q_ref, k_ref, v_ref, g_ref, b_ref, ow_ref, gain_ref, out_ref,
+    toks, outw, wq, wkv, gates, bias, keys, vals, cums, cumc, mine, att,
+    tok_send, tok_recv, ow_send, ow_recv, w_send, w_recv, p_send, p_recv, a_send, a_recv, keep,
+):
+    at = Place(depth)
+    z, y, x, c = at.z, at.y, at.x, at.c
+    home = y == c
+    seq = toks.shape[0]
+    heads = 4 * depth
+    rows = q_ref.shape[0]
+    tok = Gather(at, tok_ref, toks, tok_send, tok_recv, keep.at[0])
+    ow = Gather(at, ow_ref, outw, ow_send, ow_recv, keep.at[1])
+
+    def w_parts(head, row_block):
+        cols = pl.ds(pl.multiple_of(head * size, size), size)
+        place = pl.ds(pl.multiple_of(row_block * rows, rows), rows)
+        return (
+            (q_ref.at[:, cols], wq.at[place]),
+            (k_ref.at[:, cols], wkv.at[place, pl.ds(0, size)]),
+            (v_ref.at[:, cols], wkv.at[place, pl.ds(size, size)]),
+            (g_ref, gates.at[:, place]),
+        )
+
+    away = jnp.where(home, 0, 1)
+
+    def send_w(j):
+        head = at.ahead(j)
+        return [
+            rdma(a, b, w_send.at[i, j], w_recv.at[i, j, away], head * 2 + c, at.tp)
+            for i, (a, b) in enumerate(w_parts(head, at.sp))
+        ]
+
+    def keep_w():
+        return [
+            pltpu.make_async_copy(a, b, w_recv.at[i, 0, 0])
+            for i, (a, b) in enumerate(w_parts(z, at.sp))
+        ]
+
+    def pass_w():
+        whole = ((wq, wq), (wkv, wkv), (gates, gates), (b_ref, bias))
+        return [
+            rdma(a, b, p_send.at[i], p_recv.at[i], at.sp, x * 2 + 1 - c)
+            for i, (a, b) in enumerate(whole)
+        ]
+
+    tok.begin()
+    for j in range(1, depth):
+        for copy in send_w(j):
+            copy.start()
+
+    @pl.when(home)
+    def _():
+        for copy in keep_w():
+            copy.start()
+
+    @pl.when(jnp.logical_not(home))
+    def _():
+        for copy in send_w(0):
+            copy.start()
+
+    tok.sides(0)
+    for j in range(1, depth):
+        tok.column(j)
+    ow.begin()
+    for j in range(1, depth):
+        tok.sides(j)
+    for j in range(depth):
+        tok.corner(j)
+
+    @pl.when(home)
+    def _():
+        for j in range(depth):
+            for e in range(2):
+                for i, (_a, b) in enumerate(w_parts(z, at.back(j) * 2 + (y if e == 0 else 1 - y))):
+                    pltpu.make_async_copy(b, b, w_recv.at[i, j, e]).wait()
+        for copy in pass_w():
+            copy.start()
+        moved = pltpu.make_async_copy(b_ref, bias, keep.at[2])
+        moved.start()
+        moved.wait()
+
+    tok.keep.wait()
+    for j in range(depth):
+        tok.partner(j)
+    ow.sides(0)
+    for j in range(1, depth):
+        ow.column(j)
+
+    @pl.when(jnp.logical_not(home))
+    def _():
+        for i, ref in enumerate((wq, wkv, gates, bias)):
+            pltpu.make_async_copy(ref, ref, p_recv.at[i]).wait()
+
+    raw = lax.dot_general(
+        gates[...], toks[...], (((1,), (1,)), ((), ())), preferred_element_type=jnp.float32
+    )[:8]
+    raw = raw + bias[:, :1] + math.log(seq)
+    run = jnp.minimum(raw, 0.0) - jnp.log1p(jnp.exp(-jnp.abs(raw)))
+    lane = lax.broadcasted_iota(jnp.int32, run.shape, 1)
+    step = 1
+    while step < seq:
+        run = run + jnp.where(lane >= step, pltpu.roll(run, step, 1), 0.0)
+        step *= 2
+    which = lax.broadcasted_iota(jnp.int32, run.shape, 0)
+    chosen = jnp.sum(jnp.where(which == z, run, 0.0), axis=0, keepdims=True)
+    cums[...] = jnp.broadcast_to(chosen, cums.shape)
+    cumc[...] = jnp.broadcast_to(chosen, (128, seq)).T
+
+    span = seq // (2 * depth)
+    for i in range(2 * depth):
+        part = pl.ds(i * span, span)
+        both = jnp.dot(toks[part, :], wkv[...], preferred_element_type=jnp.float32)
+        keys[part, :] = both[:, :size].astype(jnp.bfloat16)
+        vals[part, :] = both[:, size:].astype(jnp.bfloat16)
+    for j in range(1, depth):
+        ow.sides(j)
+
+    scale = size ** (-0.5)
+    own = span // 4
+    head = (2 * x + y) * depth + z
+
+    def deliver(j, dx, dc, local):
+        xx = x if dx == 0 else 1 - x
+        cc = c if dc == 0 else 1 - c
+        start = pl.multiple_of(j * span + (xx * 2 + cc) * own, own)
+        src = mine.at[pl.ds(start, own)]
+        dst = att.at[:, pl.ds(pl.multiple_of(head * size, size), size)]
+        if local:
+            return pltpu.make_async_copy(src, dst, a_recv.at[head])
+        return rdma(src, dst, a_send.at[j, dx, dc], a_recv.at[head], j * 2 + c, xx * 2 + cc)
+
+    for j in range(depth):
+        first = pl.multiple_of((2 * j + c) * span, span)
+        length = (2 * j + 2) * span
+        queries = jnp.dot(
+            toks[pl.ds(first, span), :], wq[...], preferred_element_type=jnp.float32
+        ).astype(jnp.bfloat16)
+        logits = lax.dot_general(
+            queries, keys[:length, :], (((1,), (1,)), ((), ())), preferred_element_type=jnp.float32
+        )
+        logits = logits * scale + cumc[pl.ds(first, span), :1] - cums[:1, :length]
+        key_pos = lax.broadcasted_iota(jnp.int32, logits.shape, 1)
+        query_pos = first + lax.broadcasted_iota(jnp.int32, logits.shape, 0)
+        logits = jnp.where(key_pos <= query_pos, logits, -1e30)
+        probs = jnp.exp(logits - jnp.max(logits, axis=1, keepdims=True))
+        total = jnp.sum(probs, axis=1, keepdims=True)
+        result = jnp.dot(
+            probs.astype(jnp.bfloat16), vals[:length, :], preferred_element_type=jnp.float32
+        )
+        mine[pl.ds(j * span, span), :] = (result / total).astype(jnp.bfloat16)
+        here = jnp.logical_and(home, z == j)
+        for dx in range(2):
+            for dc in range(2):
+                if dx or dc:
+                    deliver(j, dx, dc, False).start()
+
+        @pl.when(here)
+        def _():
+            deliver(j, 0, 0, True).start()
+
+        @pl.when(jnp.logical_not(here))
+        def _():
+            deliver(j, 0, 0, False).start()
+
+        ow.corner(j)
+
+    for j in range(depth):
+        ow.partner(j)
+    ow.keep.wait()
+    for h in range(heads):
+        ref = att.at[:, pl.ds(h * size, size)]
+        pltpu.make_async_copy(ref, ref, a_recv.at[h]).wait()
+
+    deep, wide = ow_ref.shape
+    pieces = []
+    for s in range(2 * depth):
+        acc = None
+        for t in range(4):
+            term = jnp.dot(
+                att[:, t * deep : (t + 1) * deep],
+                outw[(s * 4 + t) * deep : (s * 4 + t + 1) * deep, :],
+                preferred_element_type=jnp.float32,
+            )
+            acc = term if acc is None else acc + term
+        pieces.append(acc)
+    summed = jnp.concatenate(pieces, axis=1)
+    normed = summed * lax.rsqrt(jnp.mean(summed * summed, axis=-1, keepdims=True) + 1e-06)
+    out_ref[...] = (normed * gain_ref[...]).astype(jnp.bfloat16)
+
+    for copy in tok.sent + ow.sent:
+        copy.wait_send()
+    for j in range(1, depth):
+        for copy in send_w(j):
+            copy.wait_send()
+
+    @pl.when(jnp.logical_not(home))
+    def _():
+        for copy in send_w(0):
+            copy.wait_send()
+
+    @pl.when(home)
+    def _():
+        for copy in pass_w():
+            copy.wait_send()
+
+    for j in range(depth):
+        for dx in range(2):
+            for dc in range(2):
+                if dx or dc:
+                    deliver(j, dx, dc, False).wait_send()
+
+        @pl.when(jnp.logical_not(jnp.logical_and(home, z == j)))
+        def _():
+            deliver(j, 0, 0, False).wait_send()
+
+
+def head_per_chip(depth, tokens, qw, kw, vw, gw, fb, ow, gain):
+    n_sp, n_tp = lax.axis_size("sp"), lax.axis_size("tp")
+    n = n_sp * n_tp
+    own, width = tokens.shape
+    seq = own * n
+    rows = qw.shape[0]
+    size = qw.shape[1] // gw.shape[1]
+    deep, wide = ow.shape
+    gates = jnp.zeros((16, rows), jnp.bfloat16).at[: gw.shape[1]].set(gw.T)
+    bias = jnp.zeros((8, 128), jnp.float32).at[: fb.shape[0]].set(fb[:, None])
+    vm = pl.BlockSpec(memory_space=pltpu.VMEM)
+    bf, f32 = jnp.bfloat16, jnp.float32
+    dma = pltpu.SemaphoreType.DMA
+    return pl.pallas_call(
+        lambda *refs: layer(depth, size, *refs),
+        out_shape=jax.ShapeDtypeStruct((own, wide * n_sp), bf),
+        in_specs=[vm] * 8,
+        out_specs=vm,
+        scratch_shapes=[
+            pltpu.VMEM((seq, width), bf),
+            pltpu.VMEM((n * deep, wide), bf),
+            pltpu.VMEM((rows * n_sp, size), bf),
+            pltpu.VMEM((rows * n_sp, 2 * size), bf),
+            pltpu.VMEM((16, rows * n_sp), bf),
+            pltpu.VMEM((8, 128), f32),
+            pltpu.VMEM((seq, size), bf),
+            pltpu.VMEM((seq, size), bf),
+            pltpu.VMEM((8, seq), f32),
+            pltpu.VMEM((seq, 128), f32),
+            pltpu.VMEM((seq // 2, size), bf),
+            pltpu.VMEM((own, deep * n_tp), bf),
+            dma((10, depth)),
+            dma((10, depth)),
+            dma((10, depth)),
+            dma((10, depth)),
+            dma((4, depth)),
+            dma((4, depth, 2)),
+            dma((4,)),
+            dma((4,)),
+            dma((depth, 2, 2)),
+            dma((4 * depth,)),
+            dma((3,)),
+        ],
+        compiler_params=pltpu.CompilerParams(has_side_effects=True, vmem_limit_bytes=60 * 2**20),
+        name="layer",
+    )(tokens, qw, kw, vw, gates, bias, ow, gain.reshape(1, -1))
+
+
+def on_any(tokens, qw, kw, vw, gw, fb, ow, gain):
+    n_sp, n_tp = lax.axis_size("sp"), lax.axis_size("tp")
+    depth = n_sp // 2
+    fits = n_sp % 2 == 0 and n_tp == 4 and gw.shape[1] == depth and depth <= 8
+    tiles = qw.shape[1] == 128 * depth and qw.shape[0] == 128 and ow.shape[1] % 128 == 0
+    if fits and tiles:
+        return head_per_chip(depth, tokens, qw, kw, vw, gw, fb, ow, gain)
+    return on_device(tokens, qw, kw, vw, gw, fb, ow, gain)
+
+
 def solution(mesh):
     placed = (
         P(("sp", "tp"), None),
@@ -119,5 +521,5 @@
         P(),
     )
     return jax.shard_map(
-        on_device, mesh=mesh, in_specs=placed, out_specs=P(("sp", "tp"), None), check_vma=False
+        on_any, mesh=mesh, in_specs=placed, out_specs=P(("sp", "tp"), None), check_vma=False
     )

time: 314 us -> 68.6 us (0.22)
  waiting for transfers between devices: 228 us -> 0 us
  Pallas kernels: 0 us -> 64.3 us
  blocking collectives: 46.9 us -> 0 us
  between operations: 13.6 us -> 0.01 us
  matrix products: 13.5 us -> 0 us
  other arithmetic: 7.89 us -> 0 us
    all_gather x6 -> x0, waiting for transfers between devices: 198 us -> none  [the longest x2 73.8 us: over_all(): lax.all_gather(a, axis, axis=dim, tiled=True)]
    pallas_call x0 -> x1, Pallas kernels: none -> 64.3 us  [head_per_chip(): pl.pallas_call(lambda *refs: layer(depth, size, *refs), out_shape=jax.Sha...]
    all_gather x3 -> x0, blocking collectives: 46.9 us -> none  [the longest x1 22.8 us: on_device(): gates_all = lax.all_gather(log_gate, 'sp', axis=0, tiled=True)]
    reduce_scatter x1 -> x0, waiting for transfers between devices: 27.2 us -> none  [own_rows(): own = lax.psum_scatter(everything, axis, scatter_dimension=0, tiled=True)]
    dot_general x4 -> x0, matrix products: 13.5 us -> none  [the longest x1 4.63 us: update(): jnp.einsum('qhd,khd->hqk', queries, key_piece, preferred_element_type=jnp...]
    reduce_sum x2 -> x0, other arithmetic: 4.26 us -> none  [the longest x1 3.2 us: update(): new_sum = run_sum * factor + jnp.sum(probs, axis=-1)]
  transfers between devices with their start and end apart: 7 -> 0, of which waited for: 7 -> 0; matrix products, arithmetic and copies ran while one was open for 5% -> 0% of each run, Pallas kernels for 0% -> 0%
where the time goes in v1:
time: 68.6 us; the launch traced here: 67.8 us
  Pallas kernels  64.3 us (94%)
  local copies, waits for them, and re-layouts  3.5 us (5%)
    pallas_call x1, Pallas kernels, head_per_chip(): pl.pallas_call(lambda *refs: layer(depth, size, *refs), out_shape=jax.Sha...  64.3 us
    unnamed x5, local copies, waits for them, and re-layouts  2.24 us

profile of v1, /device:TPU:25, one launch (start us, length us, event | category | flops | bytes accessed | tf_op | source)
XLA Modules:
  0.0 67.8 jit_solution(8211559123891910999)
XLA Ops:
  0.0 0.0 copy-start.1
  0.0 0.7 copy-done.1
  0.7 0.0 copy-start
  0.7 0.7 scatter.14.refs_5_
  1.3 0.0 copy-done
  1.3 0.6 scatter.12.refs_4_
  1.9 64.3 %layer.1 = bf16[64,1024]{1,0:T(8,128)(2,1)} custom-call(bf16[64,1024]{1,0:T(8,128)(2,1)} %refs_0_.1, bf16[128,512]{1,0:T(8,128)(2,1)} %refs_1_.1, bf16[128,512]{1,0:T(8,128)(2,1)} %refs_2_.1, bf16[128,512]{1,0:T(8,128)(2,1)} %refs_3_.1, bf16[16,128]{1,0:T(8,128)(2,1)} %scatter.12.refs_4_, f32[8,128]{1,0:T(8,128)} %scatter.14.refs_5_, ...), custom_call_target="tpu_custom_call" | custom-call | tf_op jit(solution)/shard_map/layer/pallas_call | solution.py:467
  66.2 1.6 %copy.10 = bf16[64,1024]{1,0:T(8,128)(2,1)} copy(bf16[64,1024]{1,0:T(8,128)(2,1)} %layer.1) | data formatting | bytes 262144
  (1 shorter events, 0.0 us)
Async XLA Ops:
  0.0 0.7 copy-start.1
  0.7 0.7 %copy-start = (bf16[128,4]{0,1:T(4,128)(2,1)S(1)}, bf16[128,4]{0,1:T(4,128)(2,1)}, u32[]{:S(2)}) copy-start(bf16[128,4]{0,1:T(4,128)(2,1)} %param.16) | copy-start | bytes 3076

commit v2 on v1

--- a/solution.py
+++ b/solution.py
@@ -279,6 +279,15 @@
             rdma(a, b, p_send.at[i], p_recv.at[i], at.sp, x * 2 + 1 - c)
             for i, (a, b) in enumerate(whole)
         ]
+
+    barrier = pltpu.get_barrier_semaphore()
+    n_sp, n_tp = 2 * depth, 4
+    for ds in range(n_sp):
+        for dt in range(n_tp):
+            if ds or dt:
+                peer = {"sp": lax.rem(at.sp + ds, n_sp), "tp": lax.rem(at.tp + dt, n_tp)}
+                pl.semaphore_signal(barrier, inc=1, device_id=peer, device_id_type=MESH)
+    pl.semaphore_wait(barrier, n_sp * n_tp - 1)
 
     tok.begin()
     for j in range(1, depth):
@@ -494,7 +503,9 @@
             dma((4 * depth,)),
             dma((3,)),
         ],
-        compiler_params=pltpu.CompilerParams(has_side_effects=True, vmem_limit_bytes=60 * 2**20),
+        compiler_params=pltpu.CompilerParams(
+            collective_id=0, has_side_effects=True, vmem_limit_bytes=60 * 2**20
+        ),
         name="layer",
     )(tokens, qw, kw, vw, gates, bias, ow, gain.reshape(1, -1))
 

time: 68.6 us -> 67.8 us (0.988)
  Pallas kernels: 64.3 us -> 63.2 us
    pallas_call x1, Pallas kernels: 64.3 us -> 63.2 us  [head_per_chip(): pl.pallas_call(lambda *refs: layer(depth, size, *refs), out_shape=jax.Sha...]
where the time goes in v2:
time: 67.8 us; the launch traced here: 66.7 us
  Pallas kernels  63.2 us (93%)
  local copies, waits for them, and re-layouts  3.5 us (5%)
    pallas_call x1, Pallas kernels, head_per_chip(): pl.pallas_call(lambda *refs: layer(depth, size, *refs), out_shape=jax.Sha...  63.2 us
    unnamed x5, local copies, waits for them, and re-layouts  2.24 us

profile of v2, /device:TPU:25, one launch (start us, length us, event | category | flops | bytes accessed | tf_op | source)
XLA Modules:
  0.0 66.7 jit_solution(10381529867857998180)
XLA Ops:
  0.0 0.0 copy-start.1
  0.0 0.7 copy-done.1
  0.7 0.0 copy-start
  0.7 0.7 scatter.14.refs_5_
  1.3 0.0 copy-done
  1.3 0.6 scatter.12.refs_4_
  1.9 63.2 %layer.1 = bf16[64,1024]{1,0:T(8,128)(2,1)} custom-call(bf16[64,1024]{1,0:T(8,128)(2,1)} %refs_0_.1, bf16[128,512]{1,0:T(8,128)(2,1)} %refs_1_.1, bf16[128,512]{1,0:T(8,128)(2,1)} %refs_2_.1, bf16[128,512]{1,0:T(8,128)(2,1)} %refs_3_.1, bf16[16,128]{1,0:T(8,128)(2,1)} %scatter.12.refs_4_, f32[8,128]{1,0:T(8,128)} %scatter.14.refs_5_, ...), custom_call_target="tpu_custom_call" | custom-call | tf_op jit(solution)/shard_map/layer/pallas_call | solution.py:476
  65.1 1.6 %copy.10 = bf16[64,1024]{1,0:T(8,128)(2,1)} copy(bf16[64,1024]{1,0:T(8,128)(2,1)} %layer.1) | data formatting | bytes 262144
  (1 shorter events, 0.0 us)
Async XLA Ops:
  0.0 0.7 copy-start.1
  0.7 0.7 %copy-start = (bf16[128,4]{0,1:T(4,128)(2,1)S(1)}, bf16[128,4]{0,1:T(4,128)(2,1)}, u32[]{:S(2)}) copy-start(bf16[128,4]{0,1:T(4,128)(2,1)} %param.16) | copy-start | bytes 3076

commit v3 on v1

--- a/solution.py
+++ b/solution.py
@@ -110,7 +110,7 @@
 
 
 MESH = pl.DeviceIdType.MESH
-Z_, X_, Y_, DA, DB, PC, PX, PY, PA, PB = range(10)
+Z_, X_, Y_, DA, DB, PC, PX, PY, PA, PB, ZD = range(11)
 
 
 def rdma(src, dst, send, recv, sp, tp):
@@ -137,21 +137,30 @@
     def ahead(self, j):
         return lax.rem(self.z + j, self.depth)
 
+    def nearest(self, k):
+        pick = 0
+        for z in range(self.depth):
+            others = sorted((abs(o - z), (z - o) % self.depth) for o in range(self.depth))
+            pick = pick + jnp.where(self.z == z, others[k][1], 0)
+        return pick
+
 
 class Gather:
-    def __init__(self, at, own, buf, send, recv, local):
+    def __init__(self, at, own, buf, send, recv, local, parts):
         self.at, self.own, self.buf = at, own, buf
         self.send, self.recv, self.local = send, recv, local
         self.rows = own.shape[0]
+        self.cut = self.rows // parts
         self.sent = []
+        self.maybe = []
 
     def block(self, z, y, x, c, half=None):
         start = (((z * 2 + y) * 2 + x) * 2 + c) * self.rows
         size = self.rows
         if half is not None:
-            size = self.rows // 2
-            start = start + half * size
-        return self.buf.at[pl.ds(pl.multiple_of(start, size), size)]
+            size = self.rows - self.cut if half else self.cut
+            start = start + half * self.cut
+        return self.buf.at[pl.ds(pl.multiple_of(start, self.cut), size)]
 
     def go(self, kind, j, dst, sp, tp, src=None):
         copy = rdma(
@@ -187,14 +196,35 @@
         self.keep.start()
         self.to_x(X_, 0, mine, self.own)
         self.to_y(Y_, 0, mine, self.own)
-        for j in range(1, a.depth):
-            self.go(Z_, j, mine, a.ahead(j) * 2 + a.y, a.tp, self.own)
+        self.along(a.z < a.depth - 1, Z_, 0, mine, a.ahead(1), 1, self.own)
+        self.along(a.z > 0, ZD, 0, mine, a.back(1), a.depth - 1, self.own)
         self.to_core(PC, 0, mine, self.own)
+
+    def along(self, when, kind, j, ref, z, k, src=None):
+        a = self.at
+        copy = rdma(
+            ref if src is None else src,
+            ref,
+            self.send.at[kind, j],
+            self.recv.at[Z_, k],
+            z * 2 + a.y,
+            a.tp,
+        )
+        self.maybe.append((when, copy))
+
+        @pl.when(when)
+        def _():
+            copy.start()
 
     def column(self, j):
         a = self.at
         ref = self.block(a.back(j), a.y, a.x, a.c)
         self.arrived(Z_, j, ref)
+        below = j <= a.z
+        up = jnp.logical_and(below, a.z < a.depth - 1)
+        down = jnp.logical_and(jnp.logical_not(below), a.z > 0)
+        self.along(up, Z_, j, ref, a.ahead(1), lax.rem(j + 1, a.depth))
+        self.along(down, ZD, j, ref, a.back(1), j - 1)
         self.to_x(X_, j, ref)
         self.to_y(Y_, j, ref)
         self.to_core(PC, j, ref)
@@ -229,9 +259,13 @@
         self.arrived(PB, j, self.block(z, 1 - a.y, 1 - a.x, c, 1))
 
     def end(self):
-        self.keep.wait()
         for copy in self.sent:
             copy.wait_send()
+        for when, copy in self.maybe:
+
+            @pl.when(when)
+            def _(copy=copy):
+                copy.wait_send()
 
 
 def layer(
@@ -245,8 +279,8 @@
     seq = toks.shape[0]
     heads = 4 * depth
     rows = q_ref.shape[0]
-    tok = Gather(at, tok_ref, toks, tok_send, tok_recv, keep.at[0])
-    ow = Gather(at, ow_ref, outw, ow_send, ow_recv, keep.at[1])
+    tok = Gather(at, tok_ref, toks, tok_send, tok_recv, keep.at[0], 4)
+    ow = Gather(at, ow_ref, outw, ow_send, ow_recv, keep.at[1], 2)
 
     def w_parts(head, row_block):
         cols = pl.ds(pl.multiple_of(head * size, size), size)
@@ -280,10 +314,21 @@
             for i, (a, b) in enumerate(whole)
         ]
 
+    barrier = pltpu.get_barrier_semaphore()
+    near = [(at.sp, x * 2 + 1 - c), (at.sp, (1 - x) * 2 + c), (z * 2 + 1 - y, at.tp)]
+
+    def greet(sp, tp):
+        peer = {"sp": sp, "tp": tp}
+        pl.semaphore_signal(barrier, inc=1, device_id=peer, device_id_type=MESH)
+
+    for sp, tp in near:
+        greet(sp, tp)
+    pl.when(z > 0)(lambda: greet(at.sp - 2, at.tp))
+    pl.when(z < depth - 1)(lambda: greet(at.sp + 2, at.tp))
+    ends = jnp.where(z > 0, 1, 0) + jnp.where(z < depth - 1, 1, 0)
+    pl.semaphore_wait(barrier, len(near) + ends)
+
     tok.begin()
-    for j in range(1, depth):
-        for copy in send_w(j):
-            copy.start()
 
     @pl.when(home)
     def _():
@@ -295,14 +340,23 @@
         for copy in send_w(0):
             copy.start()
 
-    tok.sides(0)
-    for j in range(1, depth):
+    def later_w(when, j):
+        @pl.when(when)
+        def _():
+            for copy in send_w(depth - j):
+                copy.start()
+
+    order = [0] + [at.nearest(k) for k in range(1, depth)]
+    for last, j in zip(order[:-1], order[1:]):
         tok.column(j)
+        later_w(home, j)
+        tok.sides(last)
+        if last is not order[0]:
+            later_w(jnp.logical_not(home), last)
+    tok.sides(order[-1])
+    later_w(jnp.logical_not(home), order[-1])
     ow.begin()
-    for j in range(1, depth):
-        tok.sides(j)
-    for j in range(depth):
-        tok.corner(j)
+    tok.corner(order[0])
 
     @pl.when(home)
     def _():
@@ -316,12 +370,13 @@
         moved.start()
         moved.wait()
 
+    for last, j in zip(order[:-1], order[1:]):
+        tok.corner(j)
+        ow.column(j)
+        ow.sides(last)
     tok.keep.wait()
-    for j in range(depth):
+    for j in order:
         tok.partner(j)
-    ow.sides(0)
-    for j in range(1, depth):
-        ow.column(j)
 
     @pl.when(jnp.logical_not(home))
     def _():
@@ -349,8 +404,7 @@
         both = jnp.dot(toks[part, :], wkv[...], preferred_element_type=jnp.float32)
         keys[part, :] = both[:, :size].astype(jnp.bfloat16)
         vals[part, :] = both[:, size:].astype(jnp.bfloat16)
-    for j in range(1, depth):
-        ow.sides(j)
+    ow.sides(order[-1])
 
     scale = size ** (-0.5)
     own = span // 4
@@ -399,9 +453,9 @@
         def _():
             deliver(j, 0, 0, False).start()
 
-        ow.corner(j)
-
-    for j in range(depth):
+        ow.corner(order[j])
+
+    for j in order:
         ow.partner(j)
     ow.keep.wait()
     for h in range(heads):
@@ -424,8 +478,8 @@
     normed = summed * lax.rsqrt(jnp.mean(summed * summed, axis=-1, keepdims=True) + 1e-06)
     out_ref[...] = (normed * gain_ref[...]).astype(jnp.bfloat16)
 
-    for copy in tok.sent + ow.sent:
-        copy.wait_send()
+    tok.end()
+    ow.end()
     for j in range(1, depth):
         for copy in send_w(j):
             copy.wait_send()
@@ -459,8 +513,9 @@
     rows = qw.shape[0]
     size = qw.shape[1] // gw.shape[1]
     deep, wide = ow.shape
-    gates = jnp.zeros((16, rows), jnp.bfloat16).at[: gw.shape[1]].set(gw.T)
-    bias = jnp.zeros((8, 128), jnp.float32).at[: fb.shape[0]].set(fb[:, None])
+    gates = jnp.pad(gw.T, ((0, 16 - gw.shape[1]), (0, 0)))
+    spread = jnp.broadcast_to(fb[:, None], (fb.shape[0], 128))
+    bias = jnp.pad(spread, ((0, 8 - fb.shape[0]), (0, 0)))
     vm = pl.BlockSpec(memory_space=pltpu.VMEM)
     bf, f32 = jnp.bfloat16, jnp.float32
     dma = pltpu.SemaphoreType.DMA
@@ -482,10 +537,10 @@
             pltpu.VMEM((seq, 128), f32),
             pltpu.VMEM((seq // 2, size), bf),
             pltpu.VMEM((own, deep * n_tp), bf),
-            dma((10, depth)),
-            dma((10, depth)),
-            dma((10, depth)),
-            dma((10, depth)),
+            dma((11, depth)),
+            dma((11, depth)),
+            dma((11, depth)),
+            dma((11, depth)),
             dma((4, depth)),
             dma((4, depth, 2)),
             dma((4,)),
@@ -494,7 +549,9 @@
             dma((4 * depth,)),
             dma((3,)),
         ],
-        compiler_params=pltpu.CompilerParams(has_side_effects=True, vmem_limit_bytes=60 * 2**20),
+        compiler_params=pltpu.CompilerParams(
+            collective_id=0, has_side_effects=True, vmem_limit_bytes=60 * 2**20
+        ),
         name="layer",
     )(tokens, qw, kw, vw, gates, bias, ow, gain.reshape(1, -1))
 

time: 68.6 us -> 63 us (0.918)
  Pallas kernels: 64.3 us -> 59.3 us
    pallas_call x1, Pallas kernels: 64.3 us -> 59.3 us  [head_per_chip(): pl.pallas_call(lambda *refs: layer(depth, size, *refs), out_shape=jax.Sha...]
    scatter x3 -> x0, local copies, waits for them, and re-layouts: 1.26 us -> none  [the longest x2 0.66 us: head_per_chip(): bias = jnp.zeros((8, 128), jnp.float32).at[:fb.shape[0]].set(fb[:, None])]
    pad x0 -> x3, local copies, waits for them, and re-layouts: none -> 1.26 us  [the longest x2 0.66 us: head_per_chip(): bias = jnp.pad(spread, ((0, 8 - fb.shape[0]), (0, 0)))]
where the time goes in v3:
time: 63 us; the launch traced here: 62.8 us
  Pallas kernels  59.3 us (94%)
  local copies, waits for them, and re-layouts  3.5 us (6%)
    pallas_call x1, Pallas kernels, head_per_chip(): pl.pallas_call(lambda *refs: layer(depth, size, *refs), out_shape=jax.Sha...  59.3 us
    unnamed x5, local copies, waits for them, and re-layouts  2.24 us

profile of v3, /device:TPU:25, one launch (start us, length us, event | category | flops | bytes accessed | tf_op | source)
XLA Modules:
  0.0 62.8 jit_solution(10254882668061312092)
XLA Ops:
  0.0 0.0 copy-start.1
  0.0 0.7 %copy-done.1 = f32[4]{0:T(128)S(1)} copy-done((f32[4]{0:T(128)S(1)}, f32[4]{0:T(128)}, u32[]{:S(2)}) %copy-start.1) | copy-done | bytes 40
  0.7 0.0 copy-start
  0.7 0.7 %pad.12.refs_5_ = f32[8,128]{1,0:T(8,128)} broadcast(f32[8]{0:T(128)S(1)} %pad.11), dimensions={0} | broadcast | bytes 4128 | tf_op jit(solution)/shard_map/jit(_pad)/pad | solution.py:518
  1.3 0.0 copy-done
  1.3 0.6 pad.10.refs_4_
  1.9 59.3 %layer.1 = bf16[64,1024]{1,0:T(8,128)(2,1)} custom-call(bf16[64,1024]{1,0:T(8,128)(2,1)} %refs_0_.1, bf16[128,512]{1,0:T(8,128)(2,1)} %refs_1_.1, bf16[128,512]{1,0:T(8,128)(2,1)} %refs_2_.1, bf16[128,512]{1,0:T(8,128)(2,1)} %refs_3_.1, bf16[16,128]{1,0:T(8,128)(2,1)} %pad.10.refs_4_, f32[8,128]{1,0:T(8,128)} %pad.12.refs_5_, bf16[512,128]{1,0:T(8,128)(2,1)} %refs_6_.1, ...), custom_call_target="tpu_custom_call" | custom-call | tf_op jit(solution)/shard_map/layer/pallas_call | solution.py:522
  61.3 1.6 %copy.10 = bf16[64,1024]{1,0:T(8,128)(2,1)} copy(bf16[64,1024]{1,0:T(8,128)(2,1)} %layer.1) | data formatting | bytes 262144
  (1 shorter events, 0.0 us)
Async XLA Ops:
  0.0 0.7 %copy-start.1 = (f32[4]{0:T(128)S(1)}, f32[4]{0:T(128)}, u32[]{:S(2)}) copy-start(f32[4]{0:T(128)} %param.13) | copy-start | bytes 52
  0.7 0.7 %copy-start = (bf16[128,4]{0,1:T(4,128)(2,1)S(1)}, bf16[128,4]{0,1:T(4,128)(2,1)}, u32[]{:S(2)}) copy-start(bf16[128,4]{0,1:T(4,128)(2,1)} %param.12) | copy-start | bytes 3076

commit v4 on v3

--- a/solution.py
+++ b/solution.py
@@ -194,11 +194,15 @@
         mine = self.block(a.z, a.y, a.x, a.c)
         self.keep = pltpu.make_async_copy(self.own, mine, self.local)
         self.keep.start()
-        self.to_x(X_, 0, mine, self.own)
-        self.to_y(Y_, 0, mine, self.own)
         self.along(a.z < a.depth - 1, Z_, 0, mine, a.ahead(1), 1, self.own)
         self.along(a.z > 0, ZD, 0, mine, a.back(1), a.depth - 1, self.own)
         self.to_core(PC, 0, mine, self.own)
+
+    def spread(self):
+        a = self.at
+        mine = self.block(a.z, a.y, a.x, a.c)
+        self.to_x(X_, 0, mine, self.own)
+        self.to_y(Y_, 0, mine, self.own)
 
     def along(self, when, kind, j, ref, z, k, src=None):
         a = self.at
@@ -329,6 +333,7 @@
     pl.semaphore_wait(barrier, len(near) + ends)
 
     tok.begin()
+    tok.spread()
 
     @pl.when(home)
     def _():
@@ -353,9 +358,10 @@
         tok.sides(last)
         if last is not order[0]:
             later_w(jnp.logical_not(home), last)
+    ow.begin()
     tok.sides(order[-1])
     later_w(jnp.logical_not(home), order[-1])
-    ow.begin()
+    ow.spread()
     tok.corner(order[0])
 
     @pl.when(home)
@@ -371,8 +377,8 @@
         moved.wait()
 
     for last, j in zip(order[:-1], order[1:]):
+        ow.column(j)
         tok.corner(j)
-        ow.column(j)
         ow.sides(last)
     tok.keep.wait()
     for j in order:

time: 63 us -> 60.6 us (0.962)
  Pallas kernels: 59.3 us -> 56.9 us
    pallas_call x1, Pallas kernels: 59.3 us -> 56.9 us  [head_per_chip(): pl.pallas_call(lambda *refs: layer(depth, size, *refs), out_shape=jax.Sha...]
where the time goes in v4:
time: 60.6 us; the launch traced here: 60.4 us
  Pallas kernels  56.9 us (94%)
  local copies, waits for them, and re-layouts  3.5 us (6%)
    pallas_call x1, Pallas kernels, head_per_chip(): pl.pallas_call(lambda *refs: layer(depth, size, *refs), out_shape=jax.Sha...  56.9 us
    unnamed x5, local copies, waits for them, and re-layouts  2.24 us

profile of v4, /device:TPU:25, one launch (start us, length us, event | category | flops | bytes accessed | tf_op | source)
XLA Modules:
  0.0 60.4 jit_solution(2613525581630001120)
XLA Ops:
  0.0 0.0 copy-start.1
  0.0 0.7 %copy-done.1 = f32[4]{0:T(128)S(1)} copy-done((f32[4]{0:T(128)S(1)}, f32[4]{0:T(128)}, u32[]{:S(2)}) %copy-start.1) | copy-done | bytes 40
  0.7 0.0 copy-start
  0.7 0.7 %pad.12.refs_5_ = f32[8,128]{1,0:T(8,128)} broadcast(f32[8]{0:T(128)S(1)} %pad.11), dimensions={0} | broadcast | bytes 4128 | tf_op jit(solution)/shard_map/jit(_pad)/pad | solution.py:524
  1.3 0.0 copy-done
  1.3 0.6 pad.10.refs_4_
  1.9 56.9 %layer.1 = bf16[64,1024]{1,0:T(8,128)(2,1)} custom-call(bf16[64,1024]{1,0:T(8,128)(2,1)} %refs_0_.1, bf16[128,512]{1,0:T(8,128)(2,1)} %refs_1_.1, bf16[128,512]{1,0:T(8,128)(2,1)} %refs_2_.1, bf16[128,512]{1,0:T(8,128)(2,1)} %refs_3_.1, bf16[16,128]{1,0:T(8,128)(2,1)} %pad.10.refs_4_, f32[8,128]{1,0:T(8,128)} %pad.12.refs_5_, bf16[512,128]{1,0:T(8,128)(2,1)} %refs_6_.1, ...), custom_call_target="tpu_custom_call" | custom-call | tf_op jit(solution)/shard_map/layer/pallas_call | solution.py:528
  58.9 1.6 %copy.10 = bf16[64,1024]{1,0:T(8,128)(2,1)} copy(bf16[64,1024]{1,0:T(8,128)(2,1)} %layer.1) | data formatting | bytes 262144
  (1 shorter events, 0.0 us)
Async XLA Ops:
  0.0 0.7 %copy-start.1 = (f32[4]{0:T(128)S(1)}, f32[4]{0:T(128)}, u32[]{:S(2)}) copy-start(f32[4]{0:T(128)} %param.13) | copy-start | bytes 52
  0.7 0.7 %copy-start = (bf16[128,4]{0,1:T(4,128)(2,1)S(1)}, bf16[128,4]{0,1:T(4,128)(2,1)}, u32[]{:S(2)}) copy-start(bf16[128,4]{0,1:T(4,128)(2,1)} %param.12) | copy-start | bytes 3076
